TPU v7x, 512 devices: a whole 4x8x8 slice. The times are simulated.
512 devices in a mesh: sp: 64 (over z, y), fs: 4 (over x), tp: 2 (over core).
Axes of the slice: x: 4, y: 8, z: 8, core: 2. Of those that a mesh axis runs over, the one named last changes fastest.
Arguments:
- tokens: bfloat16 [32768, 2048], P(('fs', 'sp'), 'tp'), parts along dimension 0, may hold values from -450 to 450
- documents: int32 [32768], P(('fs', 'sp')), parts along dimension 0, may hold values from 0 to 7, never falling along the last dimension, each value on 1 to 4096 neighbouring positions
- norm_gain: bfloat16 [2048], P('tp'), may hold values from 0.099609375 to 1.8984375
- out_gate_weight: bfloat16 [2048, 1024], P('sp', 'tp'), may hold values from -0.125 to 0.125
- in_gate_weight: bfloat16 [2048, 1024], P('sp', 'tp'), may hold values from -0.125 to 0.125
- value_weight: bfloat16 [2048, 1024], P('sp', 'tp'), may hold values from -0.125 to 0.125
- conv_taps: bfloat16 [3, 1024], P(None, 'tp'), may hold values from -3.5 to 3.5
- state_in_weight: bfloat16 [2048, 1024], P('sp', 'tp'), may hold values from -0.125 to 0.125
- decay_rate: float32 [64, 64], P('tp'), may hold values from 4e-05 to 2.01
- frequency: float32 [64, 64], P('tp'), may hold values from 0 to 32
- step_log: float32 [64], P('tp'), may hold values from -3.9121 to -1.6094
- input_real: float32 [64, 64, 16], P('tp'), may hold values from -1 to 1
- input_imag: float32 [64, 64, 16], P('tp'), may hold values from -1 to 1
- readout_real: float32 [64, 16, 64], P('tp'), may hold values from -0.75 to 0.75
- readout_imag: float32 [64, 16, 64], P('tp'), may hold values from -0.75 to 0.75
- skip_gain: float32 [1024], P('tp'), may hold values from -4 to 4
- conv_out_weight: bfloat16 [1024, 2048], P('tp', 'sp'), may hold values from -0.125 to 0.125
- state_out_weight: bfloat16 [1024, 2048], P('tp', 'sp'), may hold values from -0.125 to 0.125
Outputs:
- mixed: bfloat16 [32768, 2048], P(('fs', 'sp', 'tp')), parts along dimension 0
There are 4 independent parts, one for each index of `fs`. A program takes and returns all parts, laid end to end along the dimension named above; an argument that names none is the same for every part. Nothing has to cross between parts.
All inputs are finite; a program needn't handle non-finite values.
Results may differ from a plain program's by a relative error of at most 0.015.
Values may be sent and summed in bfloat16 or wider, within the bound.
A program may use at most 64 MiB of HBM per device.

v0:
```python
import math
import jax
import jax.numpy as jnp
from jax import lax
from jax.sharding import Mesh
from jax.sharding import PartitionSpec as P

TAPS = 3
SP = ("sp_0", "sp_1")
FS_SP = ("fs", "sp_0", "sp_1")
FS_SP_TP = ("fs", "sp_0", "sp_1", "tp")
EPS = 1e-06


def rows_first(arrays, axis, dims):
    turned = [jnp.moveaxis(a, dim, 0) for a, dim in zip(arrays, dims)]
    widths = [t[0].size for t in turned]
    both = jnp.concatenate([t.reshape(-1, w) for t, w in zip(turned, widths)], axis=1)
    whole = lax.all_gather(both, axis, axis=0, tiled=True)
    parts = jnp.split(whole, [sum(widths[:k]) for k in range(1, len(widths))], axis=1)
    return tuple(
        (
            jnp.moveaxis(b.reshape(-1, *t.shape[1:]), 0, dim)
            for b, t, dim in zip(parts, turned, dims)
        )
    )


def filled_with(array, identity):
    return jax.tree.map(
        lambda part, zero: jnp.zeros_like(part) + jnp.asarray(zero, part.dtype), array, identity
    )


def gathered_once(array, axis):
    leaves = jax.tree.leaves(array)
    sequence = sorted(range(len(leaves)), key=lambda k: -leaves[k].size)
    width = (1, *leaves[sequence[0]].shape)[-1]
    lines = [
        jnp.pad(leaves[k].reshape(-1), (0, -leaves[k].size % width)).reshape(-1, width)
        for k in sequence
    ]
    both, at, found = (lax.all_gather(jnp.concatenate(lines), axis), 0, {})
    for k, line in zip(sequence, lines):
        section = both[:, at : at + len(line)].reshape(len(both), -1)
        found[k] = section[:, : leaves[k].size].reshape(-1, *leaves[k].shape)
        at += len(line)
    numbers = iter(range(len(leaves)))
    return jax.tree.map(lambda _: found[next(numbers)], array)


def entering(array, axes, combine, identity):
    before = start = filled_with(array, identity)
    total = array
    for axis in reversed(axes):
        devices, here = (lax.axis_size(axis), lax.axis_index(axis))
        pieces = gathered_once(total, axis)
        inside, total = (start, start)
        for k in range(devices):
            passed = k < here
            total = combine(total, jax.tree.map(lambda part: part[k], pieces))
            inside = jax.tree.map(lambda new, old: jnp.where(passed, new, old), total, inside)
        before = combine(inside, before)
    return before


def sent_together(arrays, axis, dim, along):
    widths = [a.shape[along] for a in arrays]
    both = jnp.concatenate(arrays, axis=along)
    whole = lax.all_gather(both, axis, axis=dim, tiled=True)
    return tuple(jnp.split(whole, [sum(widths[:k]) for k in range(1, len(widths))], axis=along))


def from_behind(block, axis, distance):
    devices = range(lax.axis_size(axis))
    route = [(i - distance, i) for i in devices if i - distance in devices]
    return lax.ppermute(block, axis, route)


def cut_along(array, dim, devices):
    shape = array.shape
    parts = array.reshape(*shape[:dim], devices, shape[dim] // devices, *shape[dim + 1 :])
    return jnp.moveaxis(parts, dim, 0)


def summed_on_arrival(array, axis, dim):
    devices = lax.axis_size(axis)
    parts = lax.all_to_all(cut_along(array, dim, devices), axis, 0, 0, tiled=True)
    return jnp.sum(parts.astype(jnp.float32), axis=0)


def chain_step(earlier, later):
    dec_real, dec_imag, end_real, end_imag, first_doc, last_doc = earlier
    late_dec_real, late_dec_imag, late_end_real, late_end_imag, late_first, late_last = later
    joined = (late_first == last_doc) | (last_doc < 0.0) | (late_first < 0.0)
    link = joined.astype(jnp.float32)
    carried_real = late_dec_real * end_real - late_dec_imag * end_imag
    carried_imag = late_dec_real * end_imag + late_dec_imag * end_real
    return (
        link * (late_dec_real * dec_real - late_dec_imag * dec_imag),
        link * (late_dec_real * dec_imag + late_dec_imag * dec_real),
        late_end_real + link * carried_real,
        late_end_imag + link * carried_imag,
        jnp.where(first_doc < 0.0, late_first, first_doc),
        jnp.where(late_last < 0.0, last_doc, late_last),
    )


def ssm_constants(decay_rate, frequency, step_log, input_real, input_imag):
    step_size = jnp.exp(step_log)[:, None]
    damping = decay_rate * step_size
    turning = frequency * step_size
    fading = jnp.exp(-damping)
    coef_imag = fading * jnp.sin(turning)
    half_sine = jnp.sin(turning / 2.0)
    less_real = jnp.expm1(-damping) * jnp.cos(turning) - 2.0 * half_sine * half_sine
    denominator = decay_rate * decay_rate + frequency * frequency
    ratio_real = (-less_real * decay_rate + coef_imag * frequency) / denominator
    ratio_imag = (-coef_imag * decay_rate - less_real * frequency) / denominator
    bbar_real = ratio_real[..., None] * input_real - ratio_imag[..., None] * input_imag
    bbar_imag = ratio_real[..., None] * input_imag + ratio_imag[..., None] * input_real
    return (bbar_real, bbar_imag, damping.reshape(-1), turning.reshape(-1))


def block_recurrence(
    damping,
    turning,
    bbar_real,
    bbar_imag,
    driven,
    keep_rows,
    doc_rows,
    carry_real,
    carry_imag,
    readout_real,
    readout_imag,
):
    groups, group_size, state_size = readout_real.shape
    row_count = driven.shape[0]
    block = math.gcd(row_count, 16)
    blocks = row_count // block
    steps = jnp.arange(block, dtype=jnp.float32)
    gap = steps[:, None] - steps[None, :]
    lower = (gap >= 0.0).astype(jnp.float32)
    gap_pos = jnp.maximum(gap, 0.0)[:, :, None]
    pair_fade = jnp.exp(-gap_pos * damping[None, None, :])
    pair_real = pair_fade * jnp.cos(gap_pos * turning[None, None, :])
    pair_imag = pair_fade * jnp.sin(gap_pos * turning[None, None, :])
    lead = (steps + 1.0)[:, None]
    lead_fade = jnp.exp(-lead * damping[None, :])
    lead_real = lead_fade * jnp.cos(lead * turning[None, :])
    lead_imag = lead_fade * jnp.sin(lead * turning[None, :])

    def one_block(carry, pieces):
        start_real, start_imag = carry
        inputs, keeps, docs = pieces
        split_rows = inputs.reshape(block, groups, group_size)
        push_real = jnp.einsum("tgh,gph->tgp", split_rows, bbar_real).reshape(
            block, groups * state_size
        )
        push_imag = jnp.einsum("tgh,gph->tgp", split_rows, bbar_imag).reshape(
            block, groups * state_size
        )
        same = lower * (docs[:, None] == docs[None, :]).astype(jnp.float32)
        weigh_real = same[:, :, None] * pair_real
        weigh_imag = same[:, :, None] * pair_imag
        alive = (keeps[0] * (docs == docs[0]).astype(jnp.float32))[:, None]
        held_real = jnp.sum(
            weigh_real * push_real[None, :, :] - weigh_imag * push_imag[None, :, :], axis=1
        ) + alive * (lead_real * start_real[None, :] - lead_imag * start_imag[None, :])
        held_imag = jnp.sum(
            weigh_real * push_imag[None, :, :] + weigh_imag * push_real[None, :, :], axis=1
        ) + alive * (lead_real * start_imag[None, :] + lead_imag * start_real[None, :])
        result = jnp.einsum(
            "tgp,ghp->tgh", held_real.reshape(block, groups, state_size), readout_real
        )
        result = result - jnp.einsum(
            "tgp,ghp->tgh", held_imag.reshape(block, groups, state_size), readout_imag
        )
        return ((held_real[-1], held_imag[-1]), result.reshape(block, groups * group_size))

    _, outputs = lax.scan(
        one_block,
        (carry_real, carry_imag),
        (
            driven.reshape(blocks, block, -1),
            keep_rows.reshape(blocks, block),
            doc_rows.reshape(blocks, block),
        ),
    )
    return outputs.reshape(row_count, groups * group_size)


def shards(
    tokens,
    documents,
    norm_gain,
    out_gate_weight,
    in_gate_weight,
    value_weight,
    conv_taps,
    state_in_weight,
    decay_rate,
    frequency,
    step_log,
    input_real,
    input_imag,
    readout_real,
    readout_imag,
    skip_gain,
    conv_out_weight,
    state_out_weight,
):
    row_count = tokens.shape[0]
    groups, state_size = decay_rate.shape
    group_size = input_real.shape[2]
    whole, gains = rows_first((tokens, norm_gain), "tp", (1, 0))
    values = whole.astype(jnp.float32)
    scale = lax.rsqrt(jnp.mean(values * values, axis=1, keepdims=True) + EPS)
    normed = (values * scale * gains.astype(jnp.float32)[None, :]).astype(jnp.bfloat16)

    def add_rows(pieces):
        return tuple(
            (jnp.dot(normed, piece, preferred_element_type=jnp.float32) for piece in pieces)
        )

    bbar_real, bbar_imag, damping, turning = ssm_constants(
        decay_rate, frequency, step_log, input_real, input_imag
    )
    doc_float = documents.astype(jnp.float32)
    (driven_sum,) = add_rows((lax.all_gather(state_in_weight, SP, axis=0, tiled=True),))
    driven_wide = driven_sum.astype(jnp.bfloat16).astype(jnp.float32)
    split_rows = driven_wide.reshape(row_count, groups, group_size)
    backward = (row_count - 1 - jnp.arange(row_count)).astype(jnp.float32)[:, None]
    alive = (documents == documents[-1]).astype(jnp.float32)[:, None]
    fading = jnp.exp(-backward * damping[None, :]) * alive
    weigh_real = (fading * jnp.cos(backward * turning[None, :])).reshape(
        row_count, groups, state_size
    )
    weigh_imag = (fading * jnp.sin(backward * turning[None, :])).reshape(
        row_count, groups, state_size
    )
    moment_real = jnp.einsum("tgp,tgh->gph", weigh_real, split_rows)
    moment_imag = jnp.einsum("tgp,tgh->gph", weigh_imag, split_rows)
    end_real = jnp.sum(bbar_real * moment_real - bbar_imag * moment_imag, axis=2).reshape(-1)
    end_imag = jnp.sum(bbar_real * moment_imag + bbar_imag * moment_real, axis=2).reshape(-1)
    whole_doc = (documents[0] == documents[-1]).astype(jnp.float32)
    total_fade = jnp.exp(-row_count * damping) * whole_doc
    element = (
        total_fade * jnp.cos(row_count * turning),
        total_fade * jnp.sin(row_count * turning),
        end_real,
        end_imag,
        doc_float[:1],
        doc_float[-1:],
    )
    identity = (
        jnp.ones_like(end_real),
        jnp.zeros_like(end_real),
        jnp.zeros_like(end_real),
        jnp.zeros_like(end_real),
        jnp.full((1,), -1.0, jnp.float32),
        jnp.full((1,), -1.0, jnp.float32),
    )
    incoming = entering(element, SP, chain_step, identity)
    driven_wide, incoming = (driven_wide, incoming)
    gate_sum, inner_sum, value_sum = add_rows(
        sent_together((out_gate_weight, in_gate_weight, value_weight), SP, 0, 1)
    )
    out_gate = gate_sum.astype(jnp.bfloat16).astype(jnp.float32)
    in_gate = inner_sum.astype(jnp.bfloat16).astype(jnp.float32)
    value = value_sum.astype(jnp.bfloat16).astype(jnp.float32)
    product = (in_gate * value).astype(jnp.bfloat16)
    margin = TAPS - 1
    tail_same = documents[row_count - margin :] == documents[-1]
    tail_rows = jnp.where(
        tail_same[:, None], product[row_count - margin :], jnp.zeros_like(product[:margin])
    )
    rim_rows = from_behind(tail_rows, SP, 1)
    in_dec_real, in_dec_imag, in_real, in_imag, in_first, in_last = incoming
    padded = jnp.concatenate([rim_rows, product], axis=0)
    padded_docs = jnp.concatenate([jnp.broadcast_to(in_last, (margin,)), doc_float], axis=0)
    total = jnp.zeros(product.shape, jnp.float32)
    for index in range(TAPS):
        same_doc = (padded_docs[index : index + row_count] == doc_float).astype(jnp.float32)
        total = (
            total
            + conv_taps[index].astype(jnp.float32)[None, :]
            * padded[index : index + row_count].astype(jnp.float32)
            * same_doc[:, None]
        )
    conv_out = (out_gate * total).astype(jnp.bfloat16)
    link_first = (in_last == doc_float[:1]).astype(jnp.float32)
    keep_rows = jnp.concatenate(
        [link_first, (documents[1:] == documents[:-1]).astype(jnp.float32)], axis=0
    )
    readout = block_recurrence(
        damping,
        turning,
        bbar_real,
        bbar_imag,
        driven_wide,
        keep_rows,
        doc_float,
        in_real,
        in_imag,
        readout_real,
        readout_imag,
    )
    ssm_out = jax.nn.gelu(readout + skip_gain[None, :] * driven_wide, approximate=True).astype(
        jnp.bfloat16
    )
    conv_columns, state_columns = rows_first((conv_out_weight, state_out_weight), SP, (1, 1))
    summed = summed_on_arrival(
        (
            jnp.dot(conv_out, conv_columns, preferred_element_type=jnp.float32)
            + jnp.dot(ssm_out, state_columns, preferred_element_type=jnp.float32)
        ).astype(jnp.bfloat16),
        "tp",
        0,
    )
    return summed.astype(jnp.bfloat16)


def solution(mesh):
    torus = Mesh(
        mesh.devices.reshape(8, 8, mesh.shape["fs"], mesh.shape["tp"]), ("sp_0", "sp_1", "fs", "tp")
    )
    in_specs = (
        P(FS_SP, "tp"),
        P(FS_SP),
        P("tp"),
        P(SP, "tp"),
        P(SP, "tp"),
        P(SP, "tp"),
        P(None, "tp"),
        P(SP, "tp"),
        P("tp", None),
        P("tp", None),
        P("tp"),
        P("tp", None, None),
        P("tp", None, None),
        P("tp", None, None),
        P("tp", None, None),
        P("tp"),
        P("tp", SP),
        P("tp", SP),
    )
    out_specs = P(FS_SP_TP, None)
    return jax.shard_map(
        shards, mesh=torus, in_specs=in_specs, out_specs=out_specs, check_vma=False
    )
```

profile of v0, /device:TPU:67, one launch (start us, length us, event | category | flops | bytes accessed | tf_op | source)
XLA Modules:
  0.0 351.8 jit_solution(8348065107115574287)
XLA Ops:
  7.4 1.4 pad_maximum_fusion.3
  12.0 2.5 all_gather.24
  20.6 72.3 %all-gather.10.cloned.1.call-done = bf16[2048,512]{1,0:T(8,128)(2,1)} async-done(((bf16[32,512]{1,0:T(8,128)(2,1)}), bf16[2048,512]{1,0:T(8,128)(2,1)}) %all-gather.10.cloned.1.call-update) | async-done | bytes 2097168 | tf_op jit(solution)/shard_map/all_gather | solution.py:231
  92.8 2.1 convolution_convert_fusion
  95.0 3.8 %fusion.79 = f32[32,64,16]{1,2,0:T(8,128)S(1)} fusion(bf16[128,32,16]{0,2,1:T(8,128)(2,1)S(1)} %bitcast.596, f32[32,64]{1,0:T(8,128)S(1)} %get-tuple-element.406, f32[128]{0:T(128)S(1)} %subtract_convert_fusion, f32[128]{0:T(128)S(1)} %get-tuple-element.414, f32[32,64]{1,0:T(8,128)S(1)} %get-tuple-element.405, f32[128]{0:T(128)S(1)} %fusion.178), kind=kOutput, calls=%fused_computation.77 | convolution fusion | flops 9437184 | bytes 280064 | tf_op jit(solution)/shard_map/tgp,tgh->gph/dot_general | solution.py:244
  98.8 4.4 %add_reduce_fusion = (f32[32,64]{1,0:T(8,128)S(1)}, f32[32,64]{1,0:T(8,128)S(1)}) fusion(f32[32,64,16]{1,2,0:T(8,128)S(1)} %get-tuple-element.304, f32[32,64,16]{1,2,0:T(8,128)S(1)} %get-tuple-element.253, f32[32,64,16]{1,2,0:T(8,128)S(1)} %fusion.79, bf16[128,32,16]{0,2,1:T(8,128)(2,1)S(1)} %bitcast.597, f32[32,64]{1,0:T(8,128)S(1)} %get-tuple-element.406, ...), kind=kOutput, calls=%fused_computation.109 | convolution fusion | flops 9695232 | bytes 558592 | tf_op jit(solution)/shard_map/tgp,tgh->gph/dot_general | solution.py:243
  103.5 20.1 %all-gather.2 = f32[8,6,2048]{2,1,0:T(8,128)S(1)} all-gather(f32[1,6,2048]{2,1,0:T(8,128)S(1)} %bitcast.593), channel_id=2, replica_groups=mesh['sp_0'=8,'sp_1'=8,'fs'=4,'tp'=2] {'sp_1'}, dimensions={0}, use_global_device_ids=true | all-gather | bytes 442368 | tf_op jit(solution)/shard_map/all_gather | solution.py:43
  150.5 23.6 %all-gather.3 = f32[8,6,2048]{2,1,0:T(8,128)S(1)} all-gather(f32[1,6,2048]{2,1,0:T(8,128)S(1)} %bitcast.594), channel_id=3, replica_groups=mesh['sp_0'=8,'sp_1'=8,'fs'=4,'tp'=2] {'sp_0'}, dimensions={0}, use_global_device_ids=true | all-gather | bytes 442368 | tf_op jit(solution)/shard_map/all_gather | solution.py:43
  197.1 111.0 %while.16 = (s32[]{:T(128)}, f32[2048]{0:T(1024)S(1)}, f32[2048]{0:T(1024)S(1)}, f32[8,16,512]{2,1,0:T(8,128)S(1)}, f32[8,16]{1,0:T(8,128)S(1)}, /*index=5*/bf16...) while((s32[]{:T(128)}, f32[2048]{0:T(1024)S(1)}, ...), condition=%wide.region_6.7_spmd.clone.clone, body=%wide.region_3.6_spmd.clone.clone.sunk | while | flops 12023074 | bytes 4772677 | solution.py:182
  198.2 9.6 %fusion.233 = (f32[16,2048]{1,0:T(8,128)S(1)}, f32[16,2048]{1,0:T(8,128)S(1)}) fusion(f32[2048]{0:T(1024)S(1)} %get-tuple-element.596, f32[16,16]{1,0:T(8,128)S(1)} %get-tuple-element.597, f32[2048]{0:T(1024)S(1)} %get-tuple-element.594, f32[16,16]{1,0:T(8,128)S(1)} %get-tuple-element.595, f32[16,2048]{1,0:T(8,128)S(1)} %mul.4733, ...), kind=kLoop, calls=%fused_computation.19.clone.1 | loop fusion | flops 7274496 | bytes 543744 | tf_op jit(solution)/shard_map/while/body/eval_jaxpr/reduce_sum | solution.py:171
  212.1 9.6 %fusion.233 = (f32[16,2048]{1,0:T(8,128)S(1)}, f32[16,2048]{1,0:T(8,128)S(1)}) fusion(f32[2048]{0:T(1024)S(1)} %get-tuple-element.596, f32[16,16]{1,0:T(8,128)S(1)} %get-tuple-element.597, f32[2048]{0:T(1024)S(1)} %get-tuple-element.594, f32[16,16]{1,0:T(8,128)S(1)} %get-tuple-element.595, f32[16,2048]{1,0:T(8,128)S(1)} %mul.4733, ...), kind=kLoop, calls=%fused_computation.19.clone.1 | loop fusion | flops 7274496 | bytes 543744 | tf_op jit(solution)/shard_map/while/body/eval_jaxpr/reduce_sum | solution.py:171
  226.0 9.6 %fusion.233 = (f32[16,2048]{1,0:T(8,128)S(1)}, f32[16,2048]{1,0:T(8,128)S(1)}) fusion(f32[2048]{0:T(1024)S(1)} %get-tuple-element.596, f32[16,16]{1,0:T(8,128)S(1)} %get-tuple-element.597, f32[2048]{0:T(1024)S(1)} %get-tuple-element.594, f32[16,16]{1,0:T(8,128)S(1)} %get-tuple-element.595, f32[16,2048]{1,0:T(8,128)S(1)} %mul.4733, ...), kind=kLoop, calls=%fused_computation.19.clone.1 | loop fusion | flops 7274496 | bytes 543744 | tf_op jit(solution)/shard_map/while/body/eval_jaxpr/reduce_sum | solution.py:171
  239.9 9.6 %fusion.233 = (f32[16,2048]{1,0:T(8,128)S(1)}, f32[16,2048]{1,0:T(8,128)S(1)}) fusion(f32[2048]{0:T(1024)S(1)} %get-tuple-element.596, f32[16,16]{1,0:T(8,128)S(1)} %get-tuple-element.597, f32[2048]{0:T(1024)S(1)} %get-tuple-element.594, f32[16,16]{1,0:T(8,128)S(1)} %get-tuple-element.595, f32[16,2048]{1,0:T(8,128)S(1)} %mul.4733, ...), kind=kLoop, calls=%fused_computation.19.clone.1 | loop fusion | flops 7274496 | bytes 543744 | tf_op jit(solution)/shard_map/while/body/eval_jaxpr/reduce_sum | solution.py:171
  253.8 9.6 %fusion.233 = (f32[16,2048]{1,0:T(8,128)S(1)}, f32[16,2048]{1,0:T(8,128)S(1)}) fusion(f32[2048]{0:T(1024)S(1)} %get-tuple-element.596, f32[16,16]{1,0:T(8,128)S(1)} %get-tuple-element.597, f32[2048]{0:T(1024)S(1)} %get-tuple-element.594, f32[16,16]{1,0:T(8,128)S(1)} %get-tuple-element.595, f32[16,2048]{1,0:T(8,128)S(1)} %mul.4733, ...), kind=kLoop, calls=%fused_computation.19.clone.1 | loop fusion | flops 7274496 | bytes 543744 | tf_op jit(solution)/shard_map/while/body/eval_jaxpr/reduce_sum | solution.py:171
  267.6 9.6 %fusion.233 = (f32[16,2048]{1,0:T(8,128)S(1)}, f32[16,2048]{1,0:T(8,128)S(1)}) fusion(f32[2048]{0:T(1024)S(1)} %get-tuple-element.596, f32[16,16]{1,0:T(8,128)S(1)} %get-tuple-element.597, f32[2048]{0:T(1024)S(1)} %get-tuple-element.594, f32[16,16]{1,0:T(8,128)S(1)} %get-tuple-element.595, f32[16,2048]{1,0:T(8,128)S(1)} %mul.4733, ...), kind=kLoop, calls=%fused_computation.19.clone.1 | loop fusion | flops 7274496 | bytes 543744 | tf_op jit(solution)/shard_map/while/body/eval_jaxpr/reduce_sum | solution.py:171
  281.5 9.6 %fusion.233 = (f32[16,2048]{1,0:T(8,128)S(1)}, f32[16,2048]{1,0:T(8,128)S(1)}) fusion(f32[2048]{0:T(1024)S(1)} %get-tuple-element.596, f32[16,16]{1,0:T(8,128)S(1)} %get-tuple-element.597, f32[2048]{0:T(1024)S(1)} %get-tuple-element.594, f32[16,16]{1,0:T(8,128)S(1)} %get-tuple-element.595, f32[16,2048]{1,0:T(8,128)S(1)} %mul.4733, ...), kind=kLoop, calls=%fused_computation.19.clone.1 | loop fusion | flops 7274496 | bytes 543744 | tf_op jit(solution)/shard_map/while/body/eval_jaxpr/reduce_sum | solution.py:171
  295.4 9.6 %fusion.233 = (f32[16,2048]{1,0:T(8,128)S(1)}, f32[16,2048]{1,0:T(8,128)S(1)}) fusion(f32[2048]{0:T(1024)S(1)} %get-tuple-element.596, f32[16,16]{1,0:T(8,128)S(1)} %get-tuple-element.597, f32[2048]{0:T(1024)S(1)} %get-tuple-element.594, f32[16,16]{1,0:T(8,128)S(1)} %get-tuple-element.595, f32[16,2048]{1,0:T(8,128)S(1)} %mul.4733, ...), kind=kLoop, calls=%fused_computation.19.clone.1 | loop fusion | flops 7274496 | bytes 543744 | tf_op jit(solution)/shard_map/while/body/eval_jaxpr/reduce_sum | solution.py:171
  308.3 2.1 fusion.67
  310.4 2.1 fusion.61
  312.6 1.9 collective-permute-start
  314.6 4.4 %collective-permute-done = bf16[2,512]{1,0:T(2,128)(2,1)S(1)} collective-permute-done((bf16[2,512]{1,0:T(2,128)(2,1)S(1)}, bf16[2,512]{1,0:T(2,128)(2,1)S(1)}, u32[]{:S(2)}, u32[]{:S(2)}) %collective-permute-start) | collective-permute-done | bytes 2080 | tf_op jit(solution)/shard_map/ppermute | solution.py:77
  319.0 3.4 fusion.32
  322.5 2.4 fusion.30
  324.9 19.6 %all_to_all.5 = bf16[2,64,2048]{2,1,0:T(8,128)(2,1)S(1)} all-to-all(bf16[2,64,2048]{2,1,0:T(8,128)(2,1)S(1)} %bitcast.586), channel_id=1, replica_groups=mesh['sp_0'=8,'sp_1'=8,'fs'=4,'tp'=2] {'tp'}, dimensions={0} | all-to-all | bytes 1048576 | tf_op jit(solution)/shard_map/all_to_all | solution.py:88
  (324 shorter events, 47.7 us)
Async XLA Ops:
  6.5 8.2 %copy-start.7 = (s32[128]{0:T(128)S(1)}, s32[128]{0:T(128)}, u32[]{:S(2)}) copy-start(s32[128]{0:T(128)} %param.21) | copy-start | bytes 1540
  6.5 12.1 %copy-start.9 = (f32[32]{0:T(128)S(1)}, f32[32]{0:T(128)}, u32[]{:S(2)}) copy-start(f32[32]{0:T(128)} %param.30) | copy-start | bytes 388
  6.5 12.1 %copy-start.5 = (f32[32,64]{1,0:T(8,128)S(1)}, f32[32,64]{1,0:T(8,128)}, u32[]{:S(2)}) copy-start(f32[32,64]{1,0:T(8,128)} %param.28) | copy-start | bytes 24580
  6.5 12.1 %copy-start.4 = (f32[32,64]{1,0:T(8,128)S(1)}, f32[32,64]{1,0:T(8,128)}, u32[]{:S(2)}) copy-start(f32[32,64]{1,0:T(8,128)} %param.29) | copy-start | bytes 24580
  6.5 13.8 %copy-start = (f32[32,16,64]{2,1,0:T(8,128)S(1)}, f32[32,16,64]{2,1,0:T(8,128)}, u32[]{:S(2)}) copy-start(f32[32,16,64]{2,1,0:T(8,128)} %param.33) | copy-start | bytes 393220
  6.5 13.9 %copy-start.1 = (f32[32,16,64]{2,1,0:T(8,128)S(1)}, f32[32,16,64]{2,1,0:T(8,128)}, u32[]{:S(2)}) copy-start(f32[32,16,64]{2,1,0:T(8,128)} %param.34) | copy-start | bytes 393220
  6.6 13.9 %copy-start.6 = (bf16[3,512]{1,0:T(4,128)(2,1)S(1)}, bf16[3,512]{1,0:T(4,128)(2,1)}, u32[]{:S(2)}) copy-start(bf16[3,512]{1,0:T(4,128)(2,1)} %param.26) | copy-start | bytes 9220
  6.6 13.9 %copy-start.3 = (f32[32,64,16]{1,2,0:T(8,128)S(1)}, f32[32,64,16]{1,2,0:T(8,128)}, u32[]{:S(2)}) copy-start(f32[32,64,16]{1,2,0:T(8,128)} %param.31) | copy-start | bytes 393220
  6.6 13.9 %copy-start.2 = (f32[32,64,16]{1,2,0:T(8,128)S(1)}, f32[32,64,16]{1,2,0:T(8,128)}, u32[]{:S(2)}) copy-start(f32[32,64,16]{1,2,0:T(8,128)} %param.32) | copy-start | bytes 393220
  6.6 86.2 %all-gather.10.cloned.1.call-start = ((), (), s32[]{:S(2)}) async-start(), calls=%async_computation.2 | async-start | bytes 2129920 | tf_op jit(solution)/shard_map/all_gather | solution.py:231
  7.3 301.0 %all-gather.8.cloned.1.call-start = ((), (), s32[]{:S(2)}) async-start(), calls=%async_computation.1 | async-start | bytes 6389760 | tf_op jit(solution)/shard_map/all_gather | solution.py:70
  8.8 305.7 %all-gather.12.cloned.1.call-start = ((), (), s32[]{:S(2)}) async-start(), calls=%async_computation.3 | async-start | bytes 4259840 | tf_op jit(solution)/shard_map/all_gather | solution.py:19
  197.1 111.0 %copy-start.8 = (f32[512]{0:T(512)S(1)}, f32[512]{0:T(512)}, u32[]{:S(2)}) copy-start(f32[512]{0:T(512)} %param.35) | copy-start | bytes 6148
  312.6 6.4 %collective-permute-start = (bf16[2,512]{1,0:T(2,128)(2,1)S(1)}, bf16[2,512]{1,0:T(2,128)(2,1)S(1)}, u32[]{:S(2)}, u32[]{:S(2)}) collective-permute-start(bf16[2,512]{1,0:T(2,128)(2,1)S(1)} %broadcast_select_fusion.8), channel_id=1, source_target_pairs={{0,8},{8,16},{16,24},{24,32},{32,40},{40,48},{48,56},{56,64},{64,7... | collective-permute-start | bytes 6152 | tf_op jit(solution)/shard_map/ppermute | solution.py:77
Sparse Core Ops, SparseCore 0:
  10.5 82.3 all-gather.9
  95.8 93.9 all-gather.7
  192.9 81.4 all-gather.11
where the time goes:
time: 353 us; the launch traced here: 352 us
  other arithmetic  96.2 us (27%)
  waiting for transfers between devices  77.4 us (22%)
  blocking collectives  65.8 us (19%)
  between operations  60.3 us (17%)
  matrix products  26.4 us (7%)
  local copies, waits for them, and re-layouts  22.6 us (6%)
    reduce_sum x8, other arithmetic, one_block(): jnp.sum(weigh_real * push_imag[None, :, :] + weigh_imag * push_real[None,...  76.7 us
    all_gather x1, waiting for transfers between devices, shards(): lax.all_gather(state_in_weight, SP, axis=0, tiled=True)  72.3 us
    all_gather x2, blocking collectives, gathered_once(): both, at, found = (lax.all_gather(jnp.concatenate(lines), axis), 0, {})  43.7 us
    all_to_all x1, blocking collectives, summed_on_arrival(): lax.all_to_all(cut_along(array, dim, devices), axis, 0, 0, tiled=True)  19.6 us
  transfers between devices with their start and end apart: 4, of which 2 were waited for; matrix products, arithmetic and copies ran while one was open for 39% of the time, Pallas kernels for 0%

commit v1 on v0

--- a/solution.py
+++ b/solution.py
@@ -228,7 +228,13 @@
         decay_rate, frequency, step_log, input_real, input_imag
     )
     doc_float = documents.astype(jnp.float32)
-    (driven_sum,) = add_rows((lax.all_gather(state_in_weight, SP, axis=0, tiled=True),))
+
+    def _replace_pairs_all(chunk):
+        return jnp.concatenate(
+            lax.all_to_all(jnp.stack([chunk for _ in range(lax.axis_size(SP))], 0), SP, 0, 0), 0
+        )
+
+    (driven_sum,) = add_rows((_replace_pairs_all(state_in_weight),))
     driven_wide = driven_sum.astype(jnp.bfloat16).astype(jnp.float32)
     split_rows = driven_wide.reshape(row_count, groups, group_size)
     backward = (row_count - 1 - jnp.arange(row_count)).astype(jnp.float32)[:, None]

time: 353 us -> 337 us (0.955)
  waiting for transfers between devices: 77.4 us -> 41.7 us
  starting transfers between devices: 2.03 us -> 20.2 us
    all_gather x1 -> x0, waiting for transfers between devices: 72.3 us -> none  [shards(): lax.all_gather(state_in_weight, SP, axis=0, tiled=True)]
    all_to_all x0 -> x1, waiting for transfers between devices: none -> 39.8 us  [_replace_pairs_all(): lax.all_to_all(jnp.stack([chunk for _ in range(lax.axis_size(SP))], 0), S...]
    all_to_all x0 -> x1, starting transfers between devices: none -> 15.6 us  [_replace_pairs_all(): lax.all_to_all(jnp.stack([chunk for _ in range(lax.axis_size(SP))], 0), S...]
    all_gather x2, blocking collectives: 43.7 us -> 40 us  [gathered_once(): both, at, found = (lax.all_gather(jnp.concatenate(lines), axis), 0, {})]
  transfers between devices with their start and end apart: 4 -> 4, of which waited for: 2 -> 2; matrix products, arithmetic and copies ran while one was open for 39% -> 41% of each run, Pallas kernels for 0% -> 0%
where the time goes in v1:
time: 337 us; the launch traced here: 336 us
  other arithmetic  95.4 us (28%)
  blocking collectives  64.5 us (19%)
  between operations  61.3 us (18%)
  waiting for transfers between devices  41.7 us (12%)
  matrix products  26.5 us (8%)
  local copies, waits for them, and re-layouts  25.1 us (7%)
  starting transfers between devices  20.2 us (6%)
    reduce_sum x8, other arithmetic, one_block(): jnp.sum(weigh_real * push_imag[None, :, :] + weigh_imag * push_real[None,...  76.7 us
    all_gather x2, blocking collectives, gathered_once(): both, at, found = (lax.all_gather(jnp.concatenate(lines), axis), 0, {})  40 us
    all_to_all x1, waiting for transfers between devices, _replace_pairs_all(): lax.all_to_all(jnp.stack([chunk for _ in range(lax.axis_size(SP))], 0), S...  39.8 us
    all_to_all x1, blocking collectives, summed_on_arrival(): lax.all_to_all(cut_along(array, dim, devices), axis, 0, 0, tiled=True)  21.4 us
    all_to_all x1, starting transfers between devices, _replace_pairs_all(): lax.all_to_all(jnp.stack([chunk for _ in range(lax.axis_size(SP))], 0), S...  15.6 us
    add x16, other arithmetic, one_block(): jnp.sum(weigh_real * push_imag[None, :, :] + weigh_imag * push_real[None,...  6.99 us
  transfers between devices with their start and end apart: 4, of which 2 were waited for; matrix products, arithmetic and copies ran while one was open for 41% of the time, Pallas kernels for 0%

profile of v1, /device:TPU:67, one launch (start us, length us, event | category | flops | bytes accessed | tf_op | source)
XLA Modules:
  0.0 335.7 jit_solution(5770984685856397555)
XLA Ops:
  8.0 2.3 stack.2
  10.4 15.6 %all-to-all-start = ((bf16[64,32,512]{2,1,0:T(8,128)(2,1)}), bf16[64,32,512]{2,1,0:T(8,128)(2,1)}, u32[]{:S(2)}, u32[]{:S(2)}) async-start(bf16[64,32,512]{2,1,0:T(8,128)(2,1)} %stack.2), calls=%async_computation | async-start | bytes 4194304 | tf_op jit(solution)/shard_map/all_to_all | solution.py:234
  31.6 3.1 all_gather.21
  36.5 39.8 %all-to-all-done = bf16[64,32,512]{2,1,0:T(8,128)(2,1)} async-done(((bf16[64,32,512]{2,1,0:T(8,128)(2,1)}), bf16[64,32,512]{2,1,0:T(8,128)(2,1)}, u32[]{:S(2)}, u32[]{:S(2)}) %all-to-all-start) | async-done | bytes 2097184 | tf_op jit(solution)/shard_map/all_to_all | solution.py:234
  76.3 2.1 convolution_convert_fusion
  78.6 3.8 %fusion.79 = f32[32,64,16]{1,2,0:T(8,128)S(1)} fusion(bf16[128,32,16]{0,2,1:T(8,128)(2,1)S(1)} %bitcast.597, f32[32,64]{1,0:T(8,128)S(1)} %get-tuple-element.406, f32[128]{0:T(128)S(1)} %subtract_convert_fusion, f32[128]{0:T(128)S(1)} %get-tuple-element.414, f32[32,64]{1,0:T(8,128)S(1)} %get-tuple-element.405, f32[128]{0:T(128)S(1)} %fusion.178), kind=kOutput, calls=%fused_computation.77 | convolution fusion | flops 9437184 | bytes 280064 | tf_op jit(solution)/shard_map/tgp,tgh->gph/dot_general | solution.py:250
  82.4 4.4 %add_reduce_fusion = (f32[32,64]{1,0:T(8,128)S(1)}, f32[32,64]{1,0:T(8,128)S(1)}) fusion(f32[32,64,16]{1,2,0:T(8,128)S(1)} %get-tuple-element.304, f32[32,64,16]{1,2,0:T(8,128)S(1)} %get-tuple-element.253, f32[32,64,16]{1,2,0:T(8,128)S(1)} %fusion.79, bf16[128,32,16]{0,2,1:T(8,128)(2,1)S(1)} %bitcast.598, f32[32,64]{1,0:T(8,128)S(1)} %get-tuple-element.406, ...), kind=kOutput, calls=%fused_computation.109 | convolution fusion | flops 9695232 | bytes 558592 | tf_op jit(solution)/shard_map/tgp,tgh->gph/dot_general | solution.py:249
  87.0 22.1 %all-gather.2 = f32[8,6,2048]{2,1,0:T(8,128)S(1)} all-gather(f32[1,6,2048]{2,1,0:T(8,128)S(1)} %bitcast.594), channel_id=2, replica_groups=mesh['sp_0'=8,'sp_1'=8,'fs'=4,'tp'=2] {'sp_1'}, dimensions={0}, use_global_device_ids=true | all-gather | bytes 442368 | tf_op jit(solution)/shard_map/all_gather | solution.py:43
  136.5 17.8 %all-gather.3 = f32[8,6,2048]{2,1,0:T(8,128)S(1)} all-gather(f32[1,6,2048]{2,1,0:T(8,128)S(1)} %bitcast.595), channel_id=3, replica_groups=mesh['sp_0'=8,'sp_1'=8,'fs'=4,'tp'=2] {'sp_0'}, dimensions={0}, use_global_device_ids=true | all-gather | bytes 442368 | tf_op jit(solution)/shard_map/all_gather | solution.py:43
  177.4 112.4 %while.16 = (s32[]{:T(128)}, f32[2048]{0:T(1024)S(1)}, f32[2048]{0:T(1024)S(1)}, f32[8,16,512]{2,1,0:T(8,128)S(1)}, f32[8,16]{1,0:T(8,128)S(1)}, /*index=5*/bf16...) while((s32[]{:T(128)}, f32[2048]{0:T(1024)S(1)}, ...), condition=%wide.region_6.7_spmd.clone.clone, body=%wide.region_3.6_spmd.clone.clone.sunk | while | flops 12023074 | bytes 4772677 | solution.py:182
  178.5 9.6 %fusion.233 = (f32[16,2048]{1,0:T(8,128)S(1)}, f32[16,2048]{1,0:T(8,128)S(1)}) fusion(f32[2048]{0:T(1024)S(1)} %get-tuple-element.596, f32[16,16]{1,0:T(8,128)S(1)} %get-tuple-element.597, f32[2048]{0:T(1024)S(1)} %get-tuple-element.594, f32[16,16]{1,0:T(8,128)S(1)} %get-tuple-element.595, f32[16,2048]{1,0:T(8,128)S(1)} %mul.4733, ...), kind=kLoop, calls=%fused_computation.19.clone.1 | loop fusion | flops 7274496 | bytes 543744 | tf_op jit(solution)/shard_map/while/body/eval_jaxpr/reduce_sum | solution.py:171
  192.5 9.6 %fusion.233 = (f32[16,2048]{1,0:T(8,128)S(1)}, f32[16,2048]{1,0:T(8,128)S(1)}) fusion(f32[2048]{0:T(1024)S(1)} %get-tuple-element.596, f32[16,16]{1,0:T(8,128)S(1)} %get-tuple-element.597, f32[2048]{0:T(1024)S(1)} %get-tuple-element.594, f32[16,16]{1,0:T(8,128)S(1)} %get-tuple-element.595, f32[16,2048]{1,0:T(8,128)S(1)} %mul.4733, ...), kind=kLoop, calls=%fused_computation.19.clone.1 | loop fusion | flops 7274496 | bytes 543744 | tf_op jit(solution)/shard_map/while/body/eval_jaxpr/reduce_sum | solution.py:171
  206.6 9.6 %fusion.233 = (f32[16,2048]{1,0:T(8,128)S(1)}, f32[16,2048]{1,0:T(8,128)S(1)}) fusion(f32[2048]{0:T(1024)S(1)} %get-tuple-element.596, f32[16,16]{1,0:T(8,128)S(1)} %get-tuple-element.597, f32[2048]{0:T(1024)S(1)} %get-tuple-element.594, f32[16,16]{1,0:T(8,128)S(1)} %get-tuple-element.595, f32[16,2048]{1,0:T(8,128)S(1)} %mul.4733, ...), kind=kLoop, calls=%fused_computation.19.clone.1 | loop fusion | flops 7274496 | bytes 543744 | tf_op jit(solution)/shard_map/while/body/eval_jaxpr/reduce_sum | solution.py:171
  220.7 9.6 %fusion.233 = (f32[16,2048]{1,0:T(8,128)S(1)}, f32[16,2048]{1,0:T(8,128)S(1)}) fusion(f32[2048]{0:T(1024)S(1)} %get-tuple-element.596, f32[16,16]{1,0:T(8,128)S(1)} %get-tuple-element.597, f32[2048]{0:T(1024)S(1)} %get-tuple-element.594, f32[16,16]{1,0:T(8,128)S(1)} %get-tuple-element.595, f32[16,2048]{1,0:T(8,128)S(1)} %mul.4733, ...), kind=kLoop, calls=%fused_computation.19.clone.1 | loop fusion | flops 7274496 | bytes 543744 | tf_op jit(solution)/shard_map/while/body/eval_jaxpr/reduce_sum | solution.py:171
  234.7 9.6 %fusion.233 = (f32[16,2048]{1,0:T(8,128)S(1)}, f32[16,2048]{1,0:T(8,128)S(1)}) fusion(f32[2048]{0:T(1024)S(1)} %get-tuple-element.596, f32[16,16]{1,0:T(8,128)S(1)} %get-tuple-element.597, f32[2048]{0:T(1024)S(1)} %get-tuple-element.594, f32[16,16]{1,0:T(8,128)S(1)} %get-tuple-element.595, f32[16,2048]{1,0:T(8,128)S(1)} %mul.4733, ...), kind=kLoop, calls=%fused_computation.19.clone.1 | loop fusion | flops 7274496 | bytes 543744 | tf_op jit(solution)/shard_map/while/body/eval_jaxpr/reduce_sum | solution.py:171
  248.8 9.6 %fusion.233 = (f32[16,2048]{1,0:T(8,128)S(1)}, f32[16,2048]{1,0:T(8,128)S(1)}) fusion(f32[2048]{0:T(1024)S(1)} %get-tuple-element.596, f32[16,16]{1,0:T(8,128)S(1)} %get-tuple-element.597, f32[2048]{0:T(1024)S(1)} %get-tuple-element.594, f32[16,16]{1,0:T(8,128)S(1)} %get-tuple-element.595, f32[16,2048]{1,0:T(8,128)S(1)} %mul.4733, ...), kind=kLoop, calls=%fused_computation.19.clone.1 | loop fusion | flops 7274496 | bytes 543744 | tf_op jit(solution)/shard_map/while/body/eval_jaxpr/reduce_sum | solution.py:171
  262.8 9.6 %fusion.233 = (f32[16,2048]{1,0:T(8,128)S(1)}, f32[16,2048]{1,0:T(8,128)S(1)}) fusion(f32[2048]{0:T(1024)S(1)} %get-tuple-element.596, f32[16,16]{1,0:T(8,128)S(1)} %get-tuple-element.597, f32[2048]{0:T(1024)S(1)} %get-tuple-element.594, f32[16,16]{1,0:T(8,128)S(1)} %get-tuple-element.595, f32[16,2048]{1,0:T(8,128)S(1)} %mul.4733, ...), kind=kLoop, calls=%fused_computation.19.clone.1 | loop fusion | flops 7274496 | bytes 543744 | tf_op jit(solution)/shard_map/while/body/eval_jaxpr/reduce_sum | solution.py:171
  276.9 9.6 %fusion.233 = (f32[16,2048]{1,0:T(8,128)S(1)}, f32[16,2048]{1,0:T(8,128)S(1)}) fusion(f32[2048]{0:T(1024)S(1)} %get-tuple-element.596, f32[16,16]{1,0:T(8,128)S(1)} %get-tuple-element.597, f32[2048]{0:T(1024)S(1)} %get-tuple-element.594, f32[16,16]{1,0:T(8,128)S(1)} %get-tuple-element.595, f32[16,2048]{1,0:T(8,128)S(1)} %mul.4733, ...), kind=kLoop, calls=%fused_computation.19.clone.1 | loop fusion | flops 7274496 | bytes 543744 | tf_op jit(solution)/shard_map/while/body/eval_jaxpr/reduce_sum | solution.py:171
  290.0 2.1 fusion.67
  292.1 2.1 fusion.61
  294.3 4.6 %collective-permute-start = (bf16[2,512]{1,0:T(2,128)(2,1)S(1)}, bf16[2,512]{1,0:T(2,128)(2,1)S(1)}, u32[]{:S(2)}, u32[]{:S(2)}) collective-permute-start(bf16[2,512]{1,0:T(2,128)(2,1)S(1)} %broadcast_select_fusion.8), channel_id=1, source_target_pairs={{0,8},{8,16},{16,24},{24,32},{32,40},{40,48},{48,56},{56,64},{64,7... | collective-permute-start | bytes 6152 | tf_op jit(solution)/shard_map/ppermute | solution.py:77
  300.7 3.5 %fusion.32 = f32[128,2048]{1,0:T(8,128)S(1)} fusion(bf16[2048,1024]{1,0:T(8,128)(2,1)} %all-gather.9.cloned.1.call-done, bf16[2048,1536]{1,0:T(8,128)(2,1)} %all-gather.7.cloned.1.call-done, bf16[128,512]{1,0:T(8,128)(2,1)S(1)} %fusion.61, bf16[2,512]{1,0:T(2,128)(2,1)S(1)} %collective-permute-done, f32[128]{0:T(128)S(1)} %get-tuple-element.415, ...), kind=kOutput, calls=%fused_computation.48 | convolution fusion | flops 539295744 | bytes 5916672 | tf_op jit(solution)/shard_map/dot_general | solution.py:322
  304.2 2.4 fusion.30
  306.6 21.4 %all_to_all.10 = bf16[2,64,2048]{2,1,0:T(8,128)(2,1)S(1)} all-to-all(bf16[2,64,2048]{2,1,0:T(8,128)(2,1)S(1)} %bitcast.587), channel_id=1, replica_groups=mesh['sp_0'=8,'sp_1'=8,'fs'=4,'tp'=2] {'tp'}, dimensions={0} | all-to-all | bytes 1048576 | tf_op jit(solution)/shard_map/all_to_all | solution.py:88
  (332 shorter events, 49.6 us)
Async XLA Ops:
  6.5 283.5 %all-gather.7.cloned.1.call-start = ((), (), s32[]{:S(2)}) async-start(), calls=%async_computation.2 | async-start | bytes 6389760 | tf_op jit(solution)/shard_map/all_gather | solution.py:70
  10.3 15.7 %copy-start.5 = (bf16[512,32]{0,1:T(8,128)(2,1)S(1)}, bf16[512,32]{0,1:T(8,128)(2,1)}, u32[]{:S(2)}) copy-start(bf16[512,32]{0,1:T(8,128)(2,1)} %param.37) | copy-start | bytes 98308
  10.3 15.7 %copy-start.6 = (bf16[512,32]{0,1:T(8,128)(2,1)S(1)}, bf16[512,32]{0,1:T(8,128)(2,1)}, u32[]{:S(2)}) copy-start(bf16[512,32]{0,1:T(8,128)(2,1)} %param.36) | copy-start | bytes 98308
  10.3 16.5 %copy-start.12 = (bf16[1024]{0:T(1024)(128)(2,1)S(1)}, bf16[1024]{0:T(1024)(128)(2,1)}, u32[]{:S(2)}) copy-start(bf16[1024]{0:T(1024)(128)(2,1)} %param.22) | copy-start | bytes 6148
  10.3 16.5 %copy-start.10 = (s32[128]{0:T(128)S(1)}, s32[128]{0:T(128)}, u32[]{:S(2)}) copy-start(s32[128]{0:T(128)} %param.21) | copy-start | bytes 1540
  10.3 18.5 %copy-start.13 = (f32[32]{0:T(128)S(1)}, f32[32]{0:T(128)}, u32[]{:S(2)}) copy-start(f32[32]{0:T(128)} %param.30) | copy-start | bytes 388
  10.3 18.5 %copy-start.7 = (f32[32,64]{1,0:T(8,128)S(1)}, f32[32,64]{1,0:T(8,128)}, u32[]{:S(2)}) copy-start(f32[32,64]{1,0:T(8,128)} %param.29) | copy-start | bytes 24580
  10.3 18.5 %copy-start.8 = (f32[32,64]{1,0:T(8,128)S(1)}, f32[32,64]{1,0:T(8,128)}, u32[]{:S(2)}) copy-start(f32[32,64]{1,0:T(8,128)} %param.28) | copy-start | bytes 24580
  10.3 21.1 %copy-start = (f32[32,16,64]{2,1,0:T(8,128)S(1)}, f32[32,16,64]{2,1,0:T(8,128)}, u32[]{:S(2)}) copy-start(f32[32,16,64]{2,1,0:T(8,128)} %param.33) | copy-start | bytes 393220
  10.4 21.2 %copy-start.1 = (f32[32,16,64]{2,1,0:T(8,128)S(1)}, f32[32,16,64]{2,1,0:T(8,128)}, u32[]{:S(2)}) copy-start(f32[32,16,64]{2,1,0:T(8,128)} %param.34) | copy-start | bytes 393220
  10.4 21.2 %copy-start.2 = (bf16[128,1024]{1,0:T(8,128)(2,1)S(1)}, bf16[128,1024]{1,0:T(8,128)(2,1)}, u32[]{:S(2)}) copy-start(bf16[128,1024]{1,0:T(8,128)(2,1)} %param.20) | copy-start | bytes 786436
  10.4 66.0 %all-to-all-start = ((bf16[64,32,512]{2,1,0:T(8,128)(2,1)}), bf16[64,32,512]{2,1,0:T(8,128)(2,1)}, u32[]{:S(2)}, u32[]{:S(2)}) async-start(bf16[64,32,512]{2,1,0:T(8,128)(2,1)} %stack.2), calls=%async_computation | async-start | bytes 4194304 | tf_op jit(solution)/shard_map/all_to_all | solution.py:234
  26.0 10.4 %copy-start.9 = (bf16[3,512]{1,0:T(4,128)(2,1)S(1)}, bf16[3,512]{1,0:T(4,128)(2,1)}, u32[]{:S(2)}) copy-start(bf16[3,512]{1,0:T(4,128)(2,1)} %param.26) | copy-start | bytes 9220
  26.0 10.4 %copy-start.3 = (f32[32,64,16]{1,2,0:T(8,128)S(1)}, f32[32,64,16]{1,2,0:T(8,128)}, u32[]{:S(2)}) copy-start(f32[32,64,16]{1,2,0:T(8,128)} %param.32) | copy-start | bytes 393220
  26.0 10.4 %copy-start.4 = (f32[32,64,16]{1,2,0:T(8,128)S(1)}, f32[32,64,16]{1,2,0:T(8,128)}, u32[]{:S(2)}) copy-start(f32[32,64,16]{1,2,0:T(8,128)} %param.31) | copy-start | bytes 393220
  26.0 273.0 %all-gather.9.cloned.1.call-start = ((), (), s32[]{:S(2)}) async-start(), calls=%async_computation.3 | async-start | bytes 4259840 | tf_op jit(solution)/shard_map/all_gather | solution.py:19
  177.4 112.5 %copy-start.11 = (f32[512]{0:T(512)S(1)}, f32[512]{0:T(512)}, u32[]{:S(2)}) copy-start(f32[512]{0:T(512)} %param.35) | copy-start | bytes 6148
  294.3 6.4 %collective-permute-start = (bf16[2,512]{1,0:T(2,128)(2,1)S(1)}, bf16[2,512]{1,0:T(2,128)(2,1)S(1)}, u32[]{:S(2)}, u32[]{:S(2)}) collective-permute-start(bf16[2,512]{1,0:T(2,128)(2,1)S(1)} %broadcast_select_fusion.8), channel_id=1, source_target_pairs={{0,8},{8,16},{16,24},{24,32},{32,40},{40,48},{48,56},{56,64},{64,7... | collective-permute-start | bytes 6152 | tf_op jit(solution)/shard_map/ppermute | solution.py:77
Sparse Core Ops, SparseCore 0:
  10.3 128.1 all-gather.6
  141.6 81.2 all-gather.8
